TPU v7x, 512 devices: a whole 4x4x16 slice. The times are simulated.
512 devices in a mesh: sp: 128 (over z, x, core), tp: 4 (over y).
Axes of the slice: x: 4, y: 4, z: 16, core: 2. Of those that a mesh axis runs over, the one named last changes fastest.
Arguments:
- conv_gate: bfloat16 [32768, 512], P('sp', 'tp'), may hold values from -6 to 6
- conv_mix: bfloat16 [32768, 512], P('sp', 'tp'), may hold values from -6 to 6
- conv_input: bfloat16 [32768, 512], P('sp', 'tp'), may hold values from -6 to 6
- conv_taps: bfloat16 [3, 512], P(None, 'tp'), may hold values from -3.5 to 3.5
- query_rows: bfloat16 [32768, 512], P('sp', 'tp'), may hold values from -50 to 50, as said below
- key_rows: bfloat16 [32768, 512], P('sp', 'tp'), may hold values from -10 to 10, as said below
- value_rows: bfloat16 [32768, 512], P('sp', 'tp'), may hold values from -6 to 6
- lambdas: float32 [4], P('tp'), may hold values from 0.3 to 0.8
- head_gain: float32 [128], replicated, may hold values from 0.1 to 1.9
- w_out_conv: bfloat16 [512, 2048], P('tp'), may hold values from -0.1875 to 0.1875
- w_out_heads: bfloat16 [512, 2048], P('tp'), may hold values from -0.1875 to 0.1875
Outputs:
- mixed: bfloat16 [32768, 2048], P(('sp', 'tp'))
Inputs may be any that keep to these rules, and one draw needn't show every extreme that they name: `query_rows`: queries of order one; some rows may be far larger. `key_rows`: keys of order one.
All inputs are finite; a program needn't handle non-finite values.
Results may differ from a plain program's by a relative error of at most 0.013.
Values may be sent and summed in bfloat16 or wider, within the bound.
No kernel may reach another device: no remote copies, remote signals or barrier semaphores. Data moves between devices by JAX's collectives and lax.ppermute only.
A program may use at most 128 MiB of HBM per device.

v0:
```python
import math

import jax
import jax.numpy as jnp
from jax import lax
from jax.sharding import PartitionSpec as P

HEAD_QK = 64
HEAD_V = 128


def shifted(value, axis, steps):
    count = lax.axis_size(axis)
    initial, last = (max(0, -steps), min(count, count - steps))
    return lax.ppermute(value, axis, [(source, source + steps) for source in range(initial, last)])


def side_by_side(arrays, axis, dim, along):
    ends, at = ([], 0)
    for a in arrays[:-1]:
        at += a.shape[along]
        ends.append(at)
    both = jnp.concatenate(arrays, axis=along)
    return tuple(jnp.split(lax.all_gather(both, axis, axis=dim, tiled=True), ends, axis=along))


def in_blocks(x, dim, devices):
    shape = x.shape
    parts = x.reshape(*shape[:dim], devices, shape[dim] // devices, *shape[dim + 1 :])
    return jnp.moveaxis(parts, dim, 0)


def summed_on_arrival(x, axis, dim):
    parts = in_blocks(x, dim, lax.axis_size(axis))
    arrived = lax.all_to_all(parts, axis, split_axis=0, concat_axis=0, tiled=True)
    return arrived.astype(jnp.float32).sum(axis=0)


def conv_branch(conv_gate, conv_mix, conv_input, conv_taps):
    gated_in = (conv_mix.astype(jnp.float32) * conv_input.astype(jnp.float32)).astype(jnp.bfloat16)
    before = shifted(gated_in[-2:], "sp", 1)
    extended = jnp.concatenate([before, gated_in], axis=0).astype(jnp.float32)
    tap_values = conv_taps.astype(jnp.float32)
    convolved = (
        tap_values[0] * extended[:-2]
        + tap_values[1] * extended[1:-1]
        + tap_values[2] * extended[2:]
    )
    return (conv_gate.astype(jnp.float32) * convolved).astype(jnp.bfloat16)


def attention(query_rows, key_rows, value_rows, lambdas, head_gain):
    tok_rows = query_rows.shape[0]
    local_heads = query_rows.shape[1] // (2 * HEAD_QK)
    scale_qk = HEAD_QK ** (-0.5)
    query_heads = query_rows.reshape(tok_rows, local_heads, 2, HEAD_QK)
    own_first = lax.axis_index("sp") * tok_rows
    positions = own_first + jnp.arange(tok_rows, dtype=jnp.int32)
    initial = (
        jnp.full((local_heads, 2, tok_rows), -1e30, jnp.float32),
        jnp.zeros((local_heads, 2, tok_rows), jnp.float32),
        jnp.zeros((local_heads, 2, tok_rows, HEAD_V), jnp.float32),
    )
    every_key, every_value = side_by_side((key_rows, value_rows), "sp", 0, 1)
    running = initial
    shards_in = every_key.shape[0] // tok_rows
    block_rows = tok_rows * math.gcd(shards_in, 4)
    blocks_in = every_key.shape[0] // block_rows
    key_blocks = every_key.reshape(blocks_in, block_rows, 2, HEAD_QK)
    value_blocks = every_value.reshape(blocks_in, block_rows, HEAD_V)
    offsets = block_rows * jnp.arange(blocks_in, dtype=jnp.int32)

    def advance(state, entries):
        key_block, value_block, block_first = entries

        def update(previous):
            peak_val, denoms, numerator = previous
            scores = (
                jnp.einsum(
                    "bhmd,tmd->hmbt", query_heads, key_block, preferred_element_type=jnp.float32
                )
                * scale_qk
            )
            allowed = (block_first + jnp.arange(block_rows, dtype=jnp.int32))[None, :] <= positions[
                :, None
            ]
            scores = jnp.where(allowed, scores, -jnp.inf)
            new_peak = jnp.maximum(peak_val, jnp.max(scores, axis=-1))
            shrink = jnp.exp(peak_val - new_peak)
            weights = jnp.exp(scores - new_peak[..., None])
            denoms = denoms * shrink + jnp.sum(weights, axis=-1)
            numerator = numerator * shrink[..., None] + jnp.einsum(
                "hmbt,te->hmbe",
                weights.astype(jnp.bfloat16),
                value_block,
                preferred_element_type=jnp.float32,
            )
            return (new_peak, denoms, numerator)

        def unchanged(previous):
            return previous

        return (lax.cond(block_first <= own_first + tok_rows - 1, update, unchanged, state), None)

    running, _ = lax.scan(advance, running, (key_blocks, value_blocks, offsets))
    peak_val, denoms, numerator = running
    lambda_col = lambdas[:, None, None]
    merged = (
        numerator[:, 0] / denoms[:, 0, :, None]
        - lambda_col * numerator[:, 1] / denoms[:, 1, :, None]
    )
    merged = (
        merged
        * lax.rsqrt(jnp.mean(merged * merged, axis=-1, keepdims=True) + 1e-06)
        * head_gain
        * 0.8
    )
    return (
        jnp.transpose(merged, (1, 0, 2))
        .reshape(tok_rows, local_heads * HEAD_V)
        .astype(jnp.bfloat16)
    )


def shards(
    conv_gate,
    conv_mix,
    conv_input,
    conv_taps,
    query_rows,
    key_rows,
    value_rows,
    lambdas,
    head_gain,
    w_out_conv,
    w_out_heads,
):
    conv_out = conv_branch(conv_gate, conv_mix, conv_input, conv_taps)
    head_out = attention(query_rows, key_rows, value_rows, lambdas, head_gain)
    summed = summed_on_arrival(
        (
            jnp.dot(conv_out, w_out_conv, preferred_element_type=jnp.float32)
            + jnp.dot(head_out, w_out_heads, preferred_element_type=jnp.float32)
        ).astype(jnp.bfloat16),
        "tp",
        0,
    )
    return summed.astype(jnp.bfloat16)


def solution(mesh):
    placed = (
        P("sp", "tp"),
        P("sp", "tp"),
        P("sp", "tp"),
        P(None, "tp"),
        P("sp", "tp"),
        P("sp", "tp"),
        P("sp", "tp"),
        P("tp"),
        P(),
        P("tp", None),
        P("tp", None),
    )
    return jax.shard_map(
        shards, mesh=mesh, in_specs=placed, out_specs=P(("sp", "tp"), None), check_vma=False
    )
```

profile of v0, /device:TPU:480, one launch (start us, length us, event | category | flops | bytes accessed | tf_op | source)
XLA Modules:
  0.0 440.2 jit_solution(5544666752871872182)
XLA Ops:
  17.4 148.1 %all-gather.2.cloned.1.call-done = bf16[32768,256]{1,0:T(8,128)(2,1)} async-done(((bf16[256,256]{1,0:T(8,128)(2,1)}), bf16[32768,256]{1,0:T(8,128)(2,1)}) %all-gather.2.cloned.1.call-update) | async-done | bytes 16777232 | tf_op jit(solution)/shard_map/all_gather | solution.py:24
  165.4 11.3 %fusion.43 = (bf16[32768,128]{1,0:T(8,128)(2,1)}, bf16[32768,128]{1,0:T(8,128)(2,1)}) fusion(bf16[32768,256]{1,0:T(8,128)(2,1)} %all-gather.2.cloned.1.call-done), kind=kLoop, calls=%fused_computation.65 | loop fusion | bytes 33554432 | tf_op jit(solution)/shard_map/split | solution.py:24
  176.7 27.8 %reshape.211 = bf16[32,1024,2,64]{3,2,1,0:T(2,128)(2,1)} reshape(bf16[32768,128]{1,0:T(8,128)(2,1)} %get-tuple-element.276) | data formatting | bytes 16777216 | tf_op jit(solution)/shard_map/reshape | solution.py:69
  204.6 35.6 %copy.17 = bf16[32,1024,2,64]{1,3,2,0:T(8,128)(2,1)} copy(bf16[32,1024,2,64]{3,2,1,0:T(2,128)(2,1)} %reshape.211) | data formatting | bytes 16777216
  240.2 172.0 %while.17 = (s32[]{:T(128)}, f32[1,2,256]{2,1,0:T(2,128)S(1)}, f32[1,2,256]{2,1,0:T(2,128)S(1)}, f32[1,2,256,128]{3,2,1,0:T(8,128)S(1)}, s32[32]{0:T(128)S(1)}, ...) while((s32[]{:T(128)}, f32[1,2,256]{2,1,0:T(2,128)S(1)}, ...), condition=%wide.region_5.6_spmd.clone, body=%wide.region_0.5_spmd.clone.sunk | while | flops 205392640 | bytes 7976215 | solution.py:105
  247.0 4.2 conditional.3
  252.5 4.2 conditional.3
  258.0 4.2 conditional.3
  269.0 4.2 conditional.3
  280.0 4.2 conditional.3
  291.1 4.2 conditional.3
  296.6 4.2 conditional.3
  302.1 4.2 conditional.3
  307.6 4.2 conditional.3
  313.1 4.2 conditional.3
  324.1 4.2 conditional.3
  335.1 4.2 conditional.3
  346.1 4.2 conditional.3
  357.1 4.2 conditional.3
  368.2 4.2 conditional.3
  379.2 4.2 conditional.3
  390.2 4.2 conditional.3
  401.2 4.2 conditional.3
  413.1 19.3 %all_to_all.5 = bf16[4,64,2048]{2,1,0:T(8,128)(2,1)S(1)} all-to-all(bf16[4,64,2048]{2,1,0:T(8,128)(2,1)S(1)} %bitcast.87), channel_id=1, replica_groups=mesh['sp'=128,'tp'=4] {'tp'}, dimensions={0} | all-to-all | bytes 2097152 | tf_op jit(solution)/shard_map/all_to_all | solution.py:35
  (386 shorter events, 215.3 us)
Async XLA Ops:
  6.5 9.6 %copy-start = (bf16[128,2048]{1,0:T(8,128)(2,1)S(1)}, bf16[128,2048]{1,0:T(8,128)(2,1)}, u32[]{:S(2)}) copy-start(bf16[128,2048]{1,0:T(8,128)(2,1)} %param.24) | copy-start | bytes 1572868
  6.5 158.9 %all-gather.2.cloned.1.call-start = ((), (), s32[]{:S(2)}) async-start(), calls=%async_computation.1 | async-start | bytes 16908288 | tf_op jit(solution)/shard_map/all_gather | solution.py:24
  9.1 7.0 %collective-permute-start = (bf16[2,128]{1,0:T(2,128)(2,1)S(1)}, bf16[2,128]{1,0:T(2,128)(2,1)S(1)}, u32[]{:S(2)}, u32[]{:S(2)}) collective-permute-start(bf16[2,128]{1,0:T(2,128)(2,1)S(1)} %slice.44), channel_id=1, source_target_pairs={{0,4},{4,8},{8,12},{12,16},{16,20},{20,24},{24,28},{28,32},{32,36}... | collective-permute-start | bytes 1544 | tf_op jit(solution)/shard_map/ppermute | solution.py:15
  240.2 172.3 %copy-start.2 = (bf16[128,2048]{1,0:T(8,128)(2,1)S(1)}, bf16[128,2048]{1,0:T(8,128)(2,1)}, u32[]{:S(2)}) copy-start(bf16[128,2048]{1,0:T(8,128)(2,1)} %param.25) | copy-start | bytes 1572868
  240.2 172.3 %copy-start.3 = (f32[128]{0:T(128)S(1)}, f32[128]{0:T(128)}, u32[]{:S(2)}) copy-start(f32[128]{0:T(128)} %param.23) | copy-start | bytes 1540
  412.5 20.8 %copy-start.1 = (bf16[128,2048]{1,0:T(8,128)(2,1)S(1)}, bf16[128,2048]{1,0:T(8,128)(2,1)}, u32[]{:S(2)}) copy-start(bf16[128,2048]{1,0:T(8,128)(2,1)} %param.24) | copy-start | bytes 1572868
Sparse Core Ops, SparseCore 0:
  10.5 154.9 all-gather.1
where the time goes:
time: 447 us; the launch traced here: 440 us
  waiting for transfers between devices  151 us (34%)
  local copies, waits for them, and re-layouts  94.7 us (21%)
  matrix products  94.5 us (21%)
  other arithmetic  41.1 us (9%)
  loops' own time  23.7 us (5%)
  blocking collectives  19.3 us (4%)
  between operations  14.2 us (3%)
    all_gather x1, waiting for transfers between devices, side_by_side(): lax.all_gather(both, axis, axis=dim, tiled=True)  148 us
    dot_general x31, matrix products, update(): jnp.einsum('hmbt,te->hmbe', weights.astype(jnp.bfloat16), value_block, pr...  47 us
    dot_general x31, matrix products, update(): jnp.einsum('bhmd,tmd->hmbt', query_heads, key_block, preferred_element_ty...  45.7 us
    unnamed x10, local copies, waits for them, and re-layouts  36.6 us
    reshape x1, local copies, waits for them, and re-layouts, attention(): key_blocks = every_key.reshape(blocks_in, block_rows, 2, HEAD_QK)  27.8 us
    another operation x1, loops' own time, attention(): running, _ = lax.scan(advance, running, (key_blocks, value_blocks, offsets))  21.7 us
    add x31, other arithmetic, update(): block_first + jnp.arange(block_rows, dtype=jnp.int32)  20.1 us
    all_to_all x1, blocking collectives, summed_on_arrival(): lax.all_to_all(parts, axis, split_axis=0, concat_axis=0, tiled=True)  19.3 us
  transfers between devices with their start and end apart: 2, of which 2 were waited for; matrix products, arithmetic and copies ran while one was open for 1% of the time, Pallas kernels for 0%

commit v1 on v0

v1 whole, which is shorter than its diff:
```python
import math

import jax
import jax.numpy as jnp
from jax import lax
from jax.experimental import pallas as pl
from jax.experimental.pallas import tpu as pltpu
from jax.sharding import PartitionSpec as P

f32, bf16 = jnp.float32, jnp.bfloat16
HEAD_QK = 64
HEAD_V = 128
MAPS = 2
PLANES = 16
Q_STEP = 512
EARLY = 112
SCALE = HEAD_QK**-0.5 * math.log2(math.e)
LOW = -1e30
MASKED = -2e30
STAT = 16
OUT_ROWS = MAPS * (HEAD_V + STAT)
NN = (((1,), (0,)), ((), ()))


def flash_kernel(rows, first_row, resumed, last, at, q_ref, kv_ref, *refs):
    if resumed:
        m_in, acc_in, *refs = refs
    if last:
        out_ref, m_s, acc, qt, s_a, s_b, b_a, b_b = refs
    else:
        m_s, acc, qt, s_a, s_b, b_a, b_b = refs
    keys = kv_ref.shape[1]
    shards = q_ref.shape[0] // rows
    blocks = q_ref.shape[0] // Q_STEP
    z, j = at[0], at[1]

    def prepare(i, _):
        blk = q_ref[pl.ds(i * rows, rows), :].astype(f32).T * SCALE
        high = blk.astype(bf16).astype(f32)
        rest = blk - high
        for m in range(MAPS):
            lo, hi = HEAD_QK * m, HEAD_QK * (m + 1)
            qt[m, :, pl.ds(i * rows, rows)] = jnp.zeros((4 * HEAD_QK, rows), bf16)
            qt[m, lo:hi, pl.ds(i * rows, rows)] = high[lo:hi].astype(bf16)
            qt[m, 128 + lo : 128 + hi, pl.ds(i * rows, rows)] = rest[lo:hi].astype(bf16)
        return 0

    lax.fori_loop(0, shards, prepare, 0)
    if resumed:
        m_s[...] = m_in[...]
        acc[...] = acc_in[...]
    else:
        m_s[...] = jnp.full(m_s.shape, LOW, f32)
        acc[...] = jnp.zeros(acc.shape, f32)
    scores = ((s_a, b_a), (s_b, b_b))
    ahead = lax.broadcasted_iota(jnp.int32, (keys, rows), 0) - lax.broadcasted_iota(
        jnp.int32, (keys, rows), 1
    )

    def cols(b):
        return slice(b * Q_STEP, (b + 1) * Q_STEP)

    def score(i, b, diagonal):
        s_ref, b_ref = scores[b % 2]
        k = kv_ref[i, :, :128]
        k = jnp.concatenate([k, k], axis=1)
        for m in range(MAPS):
            s = lax.dot_general(k, qt[m, :, cols(b)], NN, preferred_element_type=f32)
            if diagonal:
                parts = []
                for h in range(Q_STEP // rows):
                    to = (b * (Q_STEP // rows) + h - j) * rows - first_row
                    parts.append(jnp.where(ahead <= to, s[:, h * rows : (h + 1) * rows], MASKED))
                s = jnp.concatenate(parts, axis=1)
            s_ref[m] = s
            b_ref[m] = jnp.max(s.reshape(keys // 8, 8, Q_STEP), axis=0)

    def weigh(v, b):
        s_ref, b_ref = scores[b % 2]
        for m in range(MAPS):
            old = m_s[m, :, cols(b)]
            new = jnp.maximum(old, jnp.max(b_ref[m], axis=0, keepdims=True))
            p = jnp.exp2(s_ref[m] - new[:1]).astype(bf16)
            shrink = jnp.exp2(old - new)
            m_s[m, :, cols(b)] = new
            o = lax.dot_general(v, p, NN, preferred_element_type=f32)
            acc[m, :, cols(b)] = acc[m, :, cols(b)] * shrink[:1] + o

    def values(i):
        v = kv_ref[i, :, 128:].astype(f32).T.astype(bf16)
        return jnp.concatenate([v, jnp.ones((STAT, keys), bf16)], axis=0)

    score(0, 0, False)

    def body(i, _):
        v = values(i)
        for b in range(blocks):
            if b + 1 < blocks:
                score(i, b + 1, False)
            else:
                score(i + 1, 0, False)
            weigh(v, b)
        return 0

    lax.fori_loop(0, z, body, 0)
    v = values(z)
    score(z, 0, True)
    for b in range(blocks):
        if b + 1 < blocks:
            score(z, b + 1, True)
        weigh(v, b)
    if not last:
        return

    def finish(s, _):
        for m in range(MAPS):
            a = acc[m, :, pl.ds(s * rows, rows)]
            den = jnp.maximum(a[HEAD_V : HEAD_V + 8], 1e-30)
            out_ref[s, HEAD_V * m : HEAD_V * (m + 1), :] = (a[:HEAD_V] * (1.0 / den[:1])).astype(
                bf16
            )
            rest = m_s[m, :, pl.ds(s * rows, rows)] + jnp.log2(den)
            parts = []
            for _part in range(3):
                hi = rest.astype(bf16).astype(f32)
                parts.append(hi)
                rest = rest - hi
            r = lax.broadcasted_iota(jnp.int32, rest.shape, 0)
            stat = jnp.where(r == 0, parts[0], jnp.where(r == 1, parts[1], parts[2]))
            at_row = MAPS * HEAD_V + STAT * m
            out_ref[s, at_row : at_row + STAT, :] = jnp.concatenate([stat, stat], axis=0).astype(
                bf16
            )
        return 0

    lax.fori_loop(0, shards, finish, 0)


def flash(at, q, kv, rows, first_row, state, last):
    queries = q.shape[0]
    keys = kv.shape[1]
    shapes = [(MAPS, 8, queries), (MAPS, HEAD_V + STAT, queries)]
    vmem = pl.BlockSpec(memory_space=pltpu.VMEM)
    scratch = [
        pltpu.VMEM((MAPS, 4 * HEAD_QK, queries), bf16),
        pltpu.VMEM((MAPS, keys, Q_STEP), f32),
        pltpu.VMEM((MAPS, keys, Q_STEP), f32),
        pltpu.VMEM((MAPS, 8, Q_STEP), f32),
        pltpu.VMEM((MAPS, 8, Q_STEP), f32),
    ]
    if last:
        out = jax.ShapeDtypeStruct((queries // rows, OUT_ROWS, rows), bf16)
        scratch = [pltpu.VMEM(s, f32) for s in shapes] + scratch
    else:
        out = [jax.ShapeDtypeStruct(s, f32) for s in shapes]

    def body(*refs):
        flash_kernel(rows, first_row, bool(state), last, *refs)

    return pl.pallas_call(
        body,
        out_shape=out,
        in_specs=[pl.BlockSpec(memory_space=pltpu.SMEM)] + [vmem] * (2 + len(state)),
        out_specs=vmem if last else [vmem, vmem],
        scratch_shapes=scratch,
        name="flash_last" if last else "flash_first",
    )(at, q, kv, *state)


def merge_kernel(lam, parts, gain, conv, w_conv, w_heads, out_ref):
    count, _, rows = parts.shape
    means = []
    for m in range(MAPS):
        at_row = MAPS * HEAD_V + STAT * m
        logs = []
        for d in range(count):
            stat = parts[d, at_row : at_row + STAT, :].astype(f32)
            logs.append(stat[0:1] + stat[1:2] + stat[2:3])
        peak = logs[0]
        for d in range(1, count):
            peak = jnp.maximum(peak, logs[d])
        weights = [jnp.exp2(x - peak) for x in logs]
        inverse = 1.0 / sum(weights)
        total = jnp.zeros((HEAD_V, rows), f32)
        for d in range(count):
            total += parts[d, HEAD_V * m : HEAD_V * (m + 1), :].astype(f32) * (
                weights[d] * inverse
            )
        means.append(total)
    diff = means[0] - lam[0] * means[1]
    square = jnp.mean(diff * diff, axis=0, keepdims=True)
    heads = (diff * lax.rsqrt(square + 1e-6)).T * (gain[...] * 0.8)
    out_ref[...] = (
        lax.dot_general(conv[...], w_conv[...], NN, preferred_element_type=f32)
        + lax.dot_general(heads.astype(bf16), w_heads[...], NN, preferred_element_type=f32)
    ).astype(bf16)


def merge(lambdas, parts, head_gain, conv_out, w_conv, w_heads):
    vmem = pl.BlockSpec(memory_space=pltpu.VMEM)
    return pl.pallas_call(
        merge_kernel,
        out_shape=jax.ShapeDtypeStruct((conv_out.shape[0], w_conv.shape[1]), bf16),
        in_specs=[pl.BlockSpec(memory_space=pltpu.SMEM)] + [vmem] * 5,
        out_specs=vmem,
        name="merge",
    )(lambdas, parts, head_gain[None, :], conv_out, w_conv, w_heads)


def conv_branch(conv_gate, conv_mix, conv_input, conv_taps):
    count = lax.axis_size("sp")
    gated_in = (conv_mix.astype(f32) * conv_input.astype(f32)).astype(bf16)
    before = lax.ppermute(gated_in[-2:], "sp", [(s, s + 1) for s in range(count - 1)])
    extended = jnp.concatenate([before, gated_in], axis=0).astype(f32)
    taps = conv_taps.astype(f32)
    convolved = taps[0] * extended[:-2] + taps[1] * extended[1:-1] + taps[2] * extended[2:]
    return (conv_gate.astype(f32) * convolved).astype(bf16)


def shards(
    conv_gate,
    conv_mix,
    conv_input,
    conv_taps,
    query_rows,
    key_rows,
    value_rows,
    lambdas,
    head_gain,
    w_out_conv,
    w_out_heads,
):
    rows = query_rows.shape[0]
    count = lax.axis_size("sp")
    in_plane = count // PLANES
    own = lax.axis_index("sp")
    at = jnp.stack([own // in_plane, own % in_plane]).astype(jnp.int32)
    plane = [[z * in_plane + j for j in range(in_plane)] for z in range(PLANES)]
    column = [[z * in_plane + j for z in range(PLANES)] for j in range(in_plane)]
    kv = jnp.concatenate([key_rows, value_rows], axis=1)
    late = lax.all_gather(kv[EARLY:], "sp", axis_index_groups=column)
    queries = lax.all_gather(query_rows, "sp", axis=0, tiled=True, axis_index_groups=plane)
    early = lax.all_gather(kv[:EARLY], "sp", axis_index_groups=column)
    conv_out = conv_branch(conv_gate, conv_mix, conv_input, conv_taps)
    state = flash(at, queries, early, rows, 0, (), False)
    partial_heads = flash(at, queries, late, rows, EARLY, tuple(state), True)
    arrived = lax.all_to_all(
        partial_heads, "sp", split_axis=0, concat_axis=0, tiled=True, axis_index_groups=plane
    )
    partial = merge(lambdas, arrived, head_gain, conv_out, w_out_conv, w_out_heads)
    ways = lax.axis_size("tp")
    pieces = lax.all_to_all(
        partial.reshape(ways, rows // ways, -1), "tp", split_axis=0, concat_axis=0, tiled=True
    )
    return pieces.astype(f32).sum(axis=0).astype(bf16)


def solution(mesh):
    placed = (
        P("sp", "tp"),
        P("sp", "tp"),
        P("sp", "tp"),
        P(None, "tp"),
        P("sp", "tp"),
        P("sp", "tp"),
        P("sp", "tp"),
        P("tp"),
        P(),
        P("tp", None),
        P("tp", None),
    )
    return jax.shard_map(
        shards, mesh=mesh, in_specs=placed, out_specs=P(("sp", "tp"), None), check_vma=False
    )
```

time: 447 us -> 151 us (0.34); the launches traced: 440 us -> 151 us
  waiting for transfers between devices: 151 us -> 14.9 us
  matrix products: 94.5 us -> 0 us
  local copies, waits for them, and re-layouts: 94.7 us -> 3.41 us
  blocking collectives: 19.3 us -> 69.3 us
  Pallas kernels: 0 us -> 40 us
  other arithmetic: 41.1 us -> 2.3 us
  loops' own time: 23.7 us -> 0 us
  starting transfers between devices: 1.92 us -> 6.44 us
    all_gather x1, waiting for transfers between devices: 148 us -> 1.41 us  [shards(): late = lax.all_gather(kv[EARLY:], 'sp', axis_index_groups=column)]
    dot_general x64 -> x0, matrix products: 94.5 us -> none  [the longest x31 47 us: update(): jnp.einsum('hmbt,te->hmbe', weights.astype(jnp.bfloat16), value_block, pr...]
    all_gather x0 -> x2, blocking collectives: none -> 50.4 us  [the longest x1 35.6 us: shards(): early = lax.all_gather(kv[:EARLY], 'sp', axis_index_groups=column)]
    pallas_call x0 -> x3, Pallas kernels: none -> 40 us  [the longest x2 36.3 us: flash(): pl.pallas_call(body, out_shape=out, in_specs=[pl.BlockSpec(memory_space=p...]
    unnamed x10 -> x11, local copies, waits for them, and re-layouts: 36.6 us -> 1.89 us
    reshape x1 -> x0, local copies, waits for them, and re-layouts: 27.8 us -> none  [attention(): key_blocks = every_key.reshape(blocks_in, block_rows, 2, HEAD_QK)]
    another operation x33 -> x0, loops' own time: 23.7 us -> none  [the longest x1 21.7 us: attention(): running, _ = lax.scan(advance, running, (key_blocks, value_blocks, offsets))]
    add x93 -> x0, other arithmetic: 20.8 us -> none  [the longest x31 20.1 us: update(): block_first + jnp.arange(block_rows, dtype=jnp.int32)]
  transfers between devices with their start and end apart: 2 -> 3, of which waited for: 2 -> 3; matrix products, arithmetic and copies ran while one was open for 1% -> 1% of each run, Pallas kernels for 0% -> 11%
where the time goes in v1:
time: 151 us
  blocking collectives  69.3 us (46%)
  Pallas kernels  40 us (26%)
  waiting for transfers between devices  14.9 us (10%)
  between operations  14.2 us (9%)
  starting transfers between devices  6.44 us (4%)
  local copies, waits for them, and re-layouts  3.41 us (2%)
  other arithmetic  2.3 us (2%)
    pallas_call x2, Pallas kernels, flash(): pl.pallas_call(body, out_shape=out, in_specs=[pl.BlockSpec(memory_space=p...  36.3 us
    all_gather x1, blocking collectives, shards(): early = lax.all_gather(kv[:EARLY], 'sp', axis_index_groups=column)  35.6 us
    all_to_all x1, blocking collectives, shards(): lax.all_to_all(partial.reshape(ways, rows // ways, -1), 'tp', split_axis=...  19 us
    all_gather x1, blocking collectives, shards(): lax.all_gather(query_rows, 'sp', axis=0, tiled=True, axis_index_groups=pl...  14.7 us
    all_to_all x1, waiting for transfers between devices, shards(): lax.all_to_all(partial_heads, 'sp', split_axis=0, concat_axis=0, tiled=Tr...  9.56 us
    all_to_all x1, starting transfers between devices, shards(): lax.all_to_all(partial_heads, 'sp', split_axis=0, concat_axis=0, tiled=Tr...  4.03 us
    ppermute x1, waiting for transfers between devices, conv_branch(): lax.ppermute(gated_in[-2:], 'sp', [(s, s + 1) for s in range(count - 1)])  3.91 us
    pallas_call x1, Pallas kernels, merge(): pl.pallas_call(merge_kernel, out_shape=jax.ShapeDtypeStruct((conv_out.sha...  3.69 us
  transfers between devices with their start and end apart: 3, of which 3 were waited for; matrix products, arithmetic and copies ran while one was open for 1% of the time, Pallas kernels for 11%

profile of v1, /device:TPU:480, one launch (start us, length us, event | category | flops | bytes accessed | tf_op | source)
XLA Modules:
  0.0 150.6 jit_solution(13822112448694880933)
XLA Ops:
  6.5 0.0 all-gather.4.cloned.1.call-start
  6.5 0.9 constant_dynamic-update-slice_fusion.1
  7.4 0.9 constant_dynamic-update-slice_fusion
  8.3 0.6 slice.36
  8.9 0.0 all-gather.4.cloned.1.call-update
  9.0 0.7 pad_add_fusion.refs_0_
  9.6 14.7 %all_gather.15.refs_1_ = bf16[2048,128]{1,0:T(8,128)(2,1)} all-gather(bf16[256,128]{1,0:T(8,128)(2,1)} %param.15), channel_id=1, replica_groups={{0,4,8,12,16,20,24,28},{32,36,40,44,48,52,56,60},{64,68,72,76,80,84,88,..., dimensions={0}, use_global_device_ids=true | all-gather | bytes 589824 | tf_op jit(solution)/shard_map/all_gather | solution.py:242
  24.4 35.6 %all-gather.1 = bf16[1792,256]{1,0:T(8,128)(2,1)} all-gather(bf16[112,256]{1,0:T(8,128)(2,1)S(1)} %slice.37), channel_id=3, replica_groups={{0,32,64,96,128,160,192,224,256,288,320,352,384,416,448,480},{4,36,68,1..., dimensions={0}, use_global_device_ids=true | all-gather | bytes 974848 | tf_op jit(solution)/shard_map/all_gather | solution.py:243
  60.0 17.3 %flash_first.1 = (f32[2,8,2048]{2,1,0:T(8,128)}, f32[2,144,2048]{2,1,0:T(8,128)}) custom-call(s32[2]{0:T(128)} %pad_add_fusion.refs_0_, bf16[2048,128]{1,0:T(8,128)(2,1)} %all_gather.15.refs_1_, bf16[16,112,256]{2,1,0:T(8,128)(2,1)} %bitcast.13), custom_call_target="tpu_custom_call" | custom-call | tf_op jit(solution)/shard_map/flash_first/pallas_call | solution.py:160
  77.2 1.4 all-gather.4.cloned.1.call-done
  78.7 19.1 %flash_last.1 = bf16[8,288,256]{2,1,0:T(8,128)(2,1)} custom-call(s32[2]{0:T(128)} %pad_add_fusion.refs_0_, bf16[2048,128]{1,0:T(8,128)(2,1)} %all_gather.15.refs_1_, bf16[16,144,256]{2,1,0:T(8,128)(2,1)} %bitcast.14, f32[2,8,2048]{2,1,0:T(8,128)} %get-tuple-element.7.refs_3_, f32[2,144,2048]{2,1,0:T(8,128)} %get-tuple-element.8.refs_4_), custom_call_target="tpu_custom_call" | custom-call | tf_op jit(solution)/shard_map/flash_last/pallas_call | solution.py:160
  97.7 0.0 copy-start.3
  97.7 4.0 %all-to-all-start = ((bf16[8,288,256]{2,1,0:T(8,128)(2,1)}), bf16[8,288,256]{2,1,0:T(8,128)(2,1)S(1)}, u32[]{:S(2)}, u32[]{:S(2)}) async-start(bf16[8,288,256]{2,1,0:T(8,128)(2,1)} %flash_last.1), calls=%async_computation | async-start | bytes 2359296 | tf_op jit(solution)/shard_map/all_to_all | solution.py:247
  101.8 0.0 copy-done.1
  101.8 0.0 copy-done.2
  101.8 2.4 %collective-permute-start = (bf16[2,128]{1,0:T(2,128)(2,1)S(1)}, bf16[2,128]{1,0:T(2,128)(2,1)S(1)}, u32[]{:S(2)}, u32[]{:S(2)}) collective-permute-start(bf16[2,128]{1,0:T(2,128)(2,1)S(1)} %slice.38), channel_id=1, source_target_pairs={{0,4},{4,8},{8,12},{12,16},{16,20},{20,24},{24,28},{28,32},{32,36}... | collective-permute-start | bytes 1544 | tf_op jit(solution)/shard_map/ppermute | solution.py:213
  104.2 0.0 copy-done.4
  104.9 3.9 %collective-permute-done = bf16[2,128]{1,0:T(2,128)(2,1)S(1)} collective-permute-done((bf16[2,128]{1,0:T(2,128)(2,1)S(1)}, bf16[2,128]{1,0:T(2,128)(2,1)S(1)}, u32[]{:S(2)}, u32[]{:S(2)}) %collective-permute-start) | collective-permute-done | bytes 544 | tf_op jit(solution)/shard_map/ppermute | solution.py:213
  108.9 0.7 fusion.2.conv
  109.6 9.6 %all-to-all-done.parts = bf16[8,288,256]{2,1,0:T(8,128)(2,1)S(1)} async-done(((bf16[8,288,256]{2,1,0:T(8,128)(2,1)}), bf16[8,288,256]{2,1,0:T(8,128)(2,1)S(1)}, u32[]{:S(2)}, u32[]{:S(2)}) %all-to-all-start) | async-done | bytes 1179680 | tf_op jit(solution)/shard_map/all_to_all | solution.py:247
  119.1 1.0 copy-done
  120.1 3.7 %merge.1 = bf16[256,2048]{1,0:T(8,128)(2,1)} custom-call(f32[1]{0:T(128)S(6)} %copy.13.lam, bf16[8,288,256]{2,1,0:T(8,128)(2,1)} %copy-done, f32[1,128]{1,0:T(1,128)} %bitcast.15, bf16[256,128]{1,0:T(8,128)(2,1)} %fusion.2.conv, bf16[128,2048]{1,0:T(8,128)(2,1)} %w_conv.1, bf16[128,2048]{1,0:T(8,128)(2,1)} %w_heads.1), custom_call_target="tpu_custom_call" | custom-call | tf_op jit(solution)/shard_map/merge/pallas_call | solution.py:201
  123.8 19.0 %all_to_all.10 = bf16[4,64,2048]{2,1,0:T(8,128)(2,1)S(1)} all-to-all(bf16[4,64,2048]{2,1,0:T(8,128)(2,1)} %bitcast.12), channel_id=1, replica_groups=mesh['sp'=128,'tp'=4] {'tp'}, dimensions={0} | all-to-all | bytes 2097152 | tf_op jit(solution)/shard_map/all_to_all | solution.py:252
  142.8 0.9 reduce_sum.12
  (11 shorter events, 0.1 us)
Async XLA Ops:
  6.5 72.1 %all-gather.4.cloned.1.call-start = ((), (), s32[]{:S(2)}) async-start(), calls=%async_computation.2 | async-start | bytes 1253376 | tf_op jit(solution)/shard_map/all_gather | solution.py:241
  97.7 4.1 %copy-start.1 = (bf16[256,128]{1,0:T(8,128)(2,1)S(1)}, bf16[256,128]{1,0:T(8,128)(2,1)}, u32[]{:S(2)}) copy-start(bf16[256,128]{1,0:T(8,128)(2,1)} %param.13) | copy-start | bytes 196612
  97.7 4.1 %copy-start.2 = (bf16[256,128]{1,0:T(8,128)(2,1)S(1)}, bf16[256,128]{1,0:T(8,128)(2,1)}, u32[]{:S(2)}) copy-start(bf16[256,128]{1,0:T(8,128)(2,1)} %param.12) | copy-start | bytes 196612
  97.7 6.5 %copy-start.4 = (bf16[3,128]{1,0:T(4,128)(2,1)S(1)}, bf16[3,128]{1,0:T(4,128)(2,1)}, u32[]{:S(2)}) copy-start(bf16[3,128]{1,0:T(4,128)(2,1)} %param.14) | copy-start | bytes 2308
  97.7 11.1 %copy-start.3 = (bf16[256,128]{1,0:T(8,128)(2,1)S(1)}, bf16[256,128]{1,0:T(8,128)(2,1)}, u32[]{:S(2)}) copy-start(bf16[256,128]{1,0:T(8,128)(2,1)} %param.11) | copy-start | bytes 196612
  97.7 21.4 %all-to-all-start = ((bf16[8,288,256]{2,1,0:T(8,128)(2,1)}), bf16[8,288,256]{2,1,0:T(8,128)(2,1)S(1)}, u32[]{:S(2)}, u32[]{:S(2)}) async-start(bf16[8,288,256]{2,1,0:T(8,128)(2,1)} %flash_last.1), calls=%async_computation | async-start | bytes 2359296 | tf_op jit(solution)/shard_map/all_to_all | solution.py:247
  101.8 7.0 %collective-permute-start = (bf16[2,128]{1,0:T(2,128)(2,1)S(1)}, bf16[2,128]{1,0:T(2,128)(2,1)S(1)}, u32[]{:S(2)}, u32[]{:S(2)}) collective-permute-start(bf16[2,128]{1,0:T(2,128)(2,1)S(1)} %slice.38), channel_id=1, source_target_pairs={{0,4},{4,8},{8,12},{12,16},{16,20},{20,24},{24,28},{28,32},{32,36}... | collective-permute-start | bytes 1544 | tf_op jit(solution)/shard_map/ppermute | solution.py:213
  119.1 1.0 copy-start
Sparse Core Ops, SparseCore 0:
  9.4 69.2 all-gather.3

commit v2 on v1

--- a/solution.py
+++ b/solution.py
@@ -12,7 +12,9 @@
 HEAD_V = 128
 MAPS = 2
 PLANES = 16
+CORES = 2
 Q_STEP = 512
+K_STEP = 256
 EARLY = 112
 SCALE = HEAD_QK**-0.5 * math.log2(math.e)
 LOW = -1e30
@@ -22,17 +24,43 @@
 NN = (((1,), (0,)), ((), ()))
 
 
-def flash_kernel(rows, first_row, resumed, last, at, q_ref, kv_ref, *refs):
-    if resumed:
-        m_in, acc_in, *refs = refs
+def pack_kernel(q_ref, k_ref, v_ref, early_ref, late_ref, copies_ref):
+    early_ref[:, :HEAD_V] = k_ref[:EARLY]
+    early_ref[:, HEAD_V:] = v_ref[:EARLY]
+    late_ref[:, :HEAD_V] = k_ref[EARLY:]
+    late_ref[:, HEAD_V:] = v_ref[EARLY:]
+    for i in range(copies_ref.shape[0]):
+        copies_ref[i] = q_ref[...]
+
+
+def pack(q, k, v, copies):
+    rows, width = q.shape
+    return pl.pallas_call(
+        pack_kernel,
+        out_shape=[
+            jax.ShapeDtypeStruct((EARLY, 2 * width), bf16),
+            jax.ShapeDtypeStruct((rows - EARLY, 2 * width), bf16),
+            jax.ShapeDtypeStruct((copies, rows, width), bf16),
+        ],
+        name="pack",
+    )(q, k, v)
+
+
+def flash_kernel(rows, first_row, keys_each, last, at, q_ref, kv_ref, *refs):
     if last:
-        out_ref, m_s, acc, qt, s_a, s_b, b_a, b_b = refs
+        m_hbm, acc_hbm, out_ref, m_s, acc, m_in, acc_in, sems, qt, s_a, s_b, b_a, b_b = refs
+        copies = [
+            pltpu.make_async_copy(m_hbm, m_in, sems.at[0]),
+            pltpu.make_async_copy(acc_hbm, acc_in, sems.at[1]),
+        ]
+        for copy in copies:
+            copy.start()
     else:
         m_s, acc, qt, s_a, s_b, b_a, b_b = refs
-    keys = kv_ref.shape[1]
     shards = q_ref.shape[0] // rows
     blocks = q_ref.shape[0] // Q_STEP
-    z, j = at[0], at[1]
+    lines = shards // 2
+    p, e, x, c = at[0], at[1], at[2], at[3]
 
     def prepare(i, _):
         blk = q_ref[pl.ds(i * rows, rows), :].astype(f32).T * SCALE
@@ -46,80 +74,93 @@
         return 0
 
     lax.fori_loop(0, shards, prepare, 0)
-    if resumed:
-        m_s[...] = m_in[...]
-        acc[...] = acc_in[...]
-    else:
-        m_s[...] = jnp.full(m_s.shape, LOW, f32)
-        acc[...] = jnp.zeros(acc.shape, f32)
+    m_s[...] = jnp.full(m_s.shape, LOW, f32)
+    acc[...] = jnp.zeros(acc.shape, f32)
     scores = ((s_a, b_a), (s_b, b_b))
-    ahead = lax.broadcasted_iota(jnp.int32, (keys, rows), 0) - lax.broadcasted_iota(
-        jnp.int32, (keys, rows), 1
-    )
 
     def cols(b):
         return slice(b * Q_STEP, (b + 1) * Q_STEP)
 
-    def score(i, b, diagonal):
+    def score(i, b, ahead):
         s_ref, b_ref = scores[b % 2]
-        k = kv_ref[i, :, :128]
+        k = kv_ref[pl.ds(i * K_STEP, K_STEP), :HEAD_V]
         k = jnp.concatenate([k, k], axis=1)
         for m in range(MAPS):
             s = lax.dot_general(k, qt[m, :, cols(b)], NN, preferred_element_type=f32)
-            if diagonal:
+            if ahead is not None:
                 parts = []
                 for h in range(Q_STEP // rows):
-                    to = (b * (Q_STEP // rows) + h - j) * rows - first_row
-                    parts.append(jnp.where(ahead <= to, s[:, h * rows : (h + 1) * rows], MASKED))
+                    g = b * (Q_STEP // rows) + h
+                    first = ((g // lines) * shards + (g % lines) * CORES + c) * rows
+                    parts.append(jnp.where(ahead <= first, s[:, h * rows : (h + 1) * rows], MASKED))
                 s = jnp.concatenate(parts, axis=1)
             s_ref[m] = s
-            b_ref[m] = jnp.max(s.reshape(keys // 8, 8, Q_STEP), axis=0)
+            b_ref[m] = jnp.max(s.reshape(K_STEP // 8, 8, Q_STEP), axis=0)
 
     def weigh(v, b):
         s_ref, b_ref = scores[b % 2]
         for m in range(MAPS):
             old = m_s[m, :, cols(b)]
             new = jnp.maximum(old, jnp.max(b_ref[m], axis=0, keepdims=True))
-            p = jnp.exp2(s_ref[m] - new[:1]).astype(bf16)
+            weights = jnp.exp2(s_ref[m] - new[:1]).astype(bf16)
             shrink = jnp.exp2(old - new)
             m_s[m, :, cols(b)] = new
-            o = lax.dot_general(v, p, NN, preferred_element_type=f32)
+            o = lax.dot_general(v, weights, NN, preferred_element_type=f32)
             acc[m, :, cols(b)] = acc[m, :, cols(b)] * shrink[:1] + o
 
     def values(i):
-        v = kv_ref[i, :, 128:].astype(f32).T.astype(bf16)
-        return jnp.concatenate([v, jnp.ones((STAT, keys), bf16)], axis=0)
-
-    score(0, 0, False)
+        v = kv_ref[pl.ds(i * K_STEP, K_STEP), HEAD_V:].astype(f32).T.astype(bf16)
+        return jnp.concatenate([v, jnp.ones((STAT, K_STEP), bf16)], axis=0)
+
+    whole = CORES * p * keys_each
+    full = whole // K_STEP
+    end = (whole + CORES * keys_each + K_STEP - 1) // K_STEP
+    score(0, 0, None)
 
     def body(i, _):
         v = values(i)
         for b in range(blocks):
             if b + 1 < blocks:
-                score(i, b + 1, False)
+                score(i, b + 1, None)
             else:
-                score(i + 1, 0, False)
+                score(i + 1, 0, None)
             weigh(v, b)
         return 0
 
-    lax.fori_loop(0, z, body, 0)
-    v = values(z)
-    score(z, 0, True)
-    for b in range(blocks):
-        if b + 1 < blocks:
-            score(z, b + 1, True)
-        weigh(v, b)
+    lax.fori_loop(0, full, body, 0)
+
+    def edge(i, _):
+        n = lax.broadcasted_iota(jnp.int32, (K_STEP, rows), 0) + (i * K_STEP - whole)
+        base = (e * shards + x * CORES) * rows + first_row
+        place = jnp.where(n < keys_each, n + base, n + (base + rows - keys_each))
+        place = jnp.where(n < 0, -rows, jnp.where(n < CORES * keys_each, place, 1 << 20))
+        ahead = place - lax.broadcasted_iota(jnp.int32, (K_STEP, rows), 1)
+        v = values(i)
+        score(i, 0, ahead)
+        for b in range(blocks):
+            if b + 1 < blocks:
+                score(i, b + 1, ahead)
+            weigh(v, b)
+        return 0
+
+    lax.fori_loop(full, end, edge, 0)
     if not last:
         return
+    for copy in copies:
+        copy.wait()
 
     def finish(s, _):
+        at_cols = pl.ds(s * rows, rows)
         for m in range(MAPS):
-            a = acc[m, :, pl.ds(s * rows, rows)]
+            peak = jnp.maximum(m_s[m, :, at_cols], m_in[m, :, at_cols])
+            mine = jnp.exp2(m_s[m, :, at_cols] - peak)[:1]
+            other = jnp.exp2(m_in[m, :, at_cols] - peak)[:1]
+            a = acc[m, :, at_cols] * mine + acc_in[m, :, at_cols] * other
             den = jnp.maximum(a[HEAD_V : HEAD_V + 8], 1e-30)
             out_ref[s, HEAD_V * m : HEAD_V * (m + 1), :] = (a[:HEAD_V] * (1.0 / den[:1])).astype(
                 bf16
             )
-            rest = m_s[m, :, pl.ds(s * rows, rows)] + jnp.log2(den)
+            rest = peak + jnp.log2(den)
             parts = []
             for _part in range(3):
                 hi = rest.astype(bf16).astype(f32)
@@ -136,31 +177,33 @@
     lax.fori_loop(0, shards, finish, 0)
 
 
-def flash(at, q, kv, rows, first_row, state, last):
+def flash(at, q, kv, rows, first_row, keys_each, state):
     queries = q.shape[0]
-    keys = kv.shape[1]
     shapes = [(MAPS, 8, queries), (MAPS, HEAD_V + STAT, queries)]
     vmem = pl.BlockSpec(memory_space=pltpu.VMEM)
     scratch = [
         pltpu.VMEM((MAPS, 4 * HEAD_QK, queries), bf16),
-        pltpu.VMEM((MAPS, keys, Q_STEP), f32),
-        pltpu.VMEM((MAPS, keys, Q_STEP), f32),
+        pltpu.VMEM((MAPS, K_STEP, Q_STEP), f32),
+        pltpu.VMEM((MAPS, K_STEP, Q_STEP), f32),
         pltpu.VMEM((MAPS, 8, Q_STEP), f32),
         pltpu.VMEM((MAPS, 8, Q_STEP), f32),
     ]
+    last = bool(state)
     if last:
         out = jax.ShapeDtypeStruct((queries // rows, OUT_ROWS, rows), bf16)
-        scratch = [pltpu.VMEM(s, f32) for s in shapes] + scratch
+        held = [pltpu.VMEM(s, f32) for s in shapes]
+        scratch = held + held + [pltpu.SemaphoreType.DMA((2,))] + scratch
     else:
         out = [jax.ShapeDtypeStruct(s, f32) for s in shapes]
 
     def body(*refs):
-        flash_kernel(rows, first_row, bool(state), last, *refs)
+        flash_kernel(rows, first_row, keys_each, last, *refs)
 
     return pl.pallas_call(
         body,
         out_shape=out,
-        in_specs=[pl.BlockSpec(memory_space=pltpu.SMEM)] + [vmem] * (2 + len(state)),
+        in_specs=[pl.BlockSpec(memory_space=pltpu.SMEM), vmem, vmem]
+        + [pl.BlockSpec(memory_space=pl.ANY)] * len(state),
         out_specs=vmem if last else [vmem, vmem],
         scratch_shapes=scratch,
         name="flash_last" if last else "flash_first",
@@ -232,20 +275,36 @@
 ):
     rows = query_rows.shape[0]
     count = lax.axis_size("sp")
-    in_plane = count // PLANES
+    lines = count // (PLANES * CORES)
     own = lax.axis_index("sp")
-    at = jnp.stack([own // in_plane, own % in_plane]).astype(jnp.int32)
-    plane = [[z * in_plane + j for j in range(in_plane)] for z in range(PLANES)]
-    column = [[z * in_plane + j for z in range(PLANES)] for j in range(in_plane)]
-    kv = jnp.concatenate([key_rows, value_rows], axis=1)
-    late = lax.all_gather(kv[EARLY:], "sp", axis_index_groups=column)
-    queries = lax.all_gather(query_rows, "sp", axis=0, tiled=True, axis_index_groups=plane)
-    early = lax.all_gather(kv[:EARLY], "sp", axis_index_groups=column)
+    in_plane = lines * CORES
+    z = own // in_plane
+    at = jnp.stack([z // 2, z % 2, own % in_plane // CORES, own % CORES]).astype(jnp.int32)
+
+    def place(p, e, x, c):
+        return ((2 * p + e) * lines + x) * CORES + c
+
+    peers = [
+        [place(p, e, x, c) for e in range(2) for x in range(lines)]
+        for p in range(PLANES // 2)
+        for c in range(CORES)
+    ]
+    column = [
+        [place(p, e, x, c) for p in range(PLANES // 2) for c in range(CORES)]
+        for e in range(2)
+        for x in range(lines)
+    ]
+    early, late, copies = pack(query_rows, key_rows, value_rows, 2 * lines)
+    late = lax.all_gather(late, "sp", axis=0, tiled=True, axis_index_groups=column)
+    queries = lax.all_to_all(
+        copies, "sp", split_axis=0, concat_axis=0, tiled=True, axis_index_groups=peers
+    ).reshape(2 * lines * rows, -1)
+    early = lax.all_gather(early, "sp", axis=0, tiled=True, axis_index_groups=column)
     conv_out = conv_branch(conv_gate, conv_mix, conv_input, conv_taps)
-    state = flash(at, queries, early, rows, 0, (), False)
-    partial_heads = flash(at, queries, late, rows, EARLY, tuple(state), True)
+    state = flash(at, queries, early, rows, 0, EARLY, ())
+    partial_heads = flash(at, queries, late, rows, EARLY, rows - EARLY, tuple(state))
     arrived = lax.all_to_all(
-        partial_heads, "sp", split_axis=0, concat_axis=0, tiled=True, axis_index_groups=plane
+        partial_heads, "sp", split_axis=0, concat_axis=0, tiled=True, axis_index_groups=peers
     )
     partial = merge(lambdas, arrived, head_gain, conv_out, w_out_conv, w_out_heads)
     ways = lax.axis_size("tp")

time: 151 us -> 127 us (0.84)
  blocking collectives: 69.3 us -> 45.6 us
  starting transfers between devices: 6.44 us -> 14.7 us
  Pallas kernels: 40 us -> 33.1 us
  local copies, waits for them, and re-layouts: 3.41 us -> 1.88 us
    all_gather x2 -> x1, blocking collectives: 50.4 us -> 27.3 us  [shards(): lax.all_gather(early, 'sp', axis=0, tiled=True, axis_index_groups=column)]
    ppermute x1, waiting for transfers between devices: 3.91 us -> 13.5 us  [conv_branch(): lax.ppermute(gated_in[-2:], 'sp', [(s, s + 1) for s in range(count - 1)])]
    all_to_all x1, waiting for transfers between devices: 9.56 us -> 0.01 us  [shards(): lax.all_to_all(partial_heads, 'sp', split_axis=0, concat_axis=0, tiled=Tr...]
    pallas_call x2, Pallas kernels: 36.3 us -> 27.7 us  [flash(): pl.pallas_call(body, out_shape=out, in_specs=[pl.BlockSpec(memory_space=p...]
    all_to_all x0 -> x1, starting transfers between devices: none -> 5.77 us  [shards(): lax.all_to_all(copies, 'sp', split_axis=0, concat_axis=0, tiled=True, axi...]
    all_to_all x1, starting transfers between devices: 4.03 us -> 6.89 us  [shards(): lax.all_to_all(partial_heads, 'sp', split_axis=0, concat_axis=0, tiled=Tr...]
    pallas_call x0 -> x1, Pallas kernels: none -> 1.78 us  [pack(): pl.pallas_call(pack_kernel, out_shape=[jax.ShapeDtypeStruct((EARLY, 2 * w...]
  transfers between devices with their start and end apart: 3 -> 4, of which waited for: 3 -> 2; matrix products, arithmetic and copies ran while one was open for 1% -> 1% of each run, Pallas kernels for 11% -> 10%
where the time goes in v2:
time: 127 us
  blocking collectives  45.6 us (36%)
  Pallas kernels  33.1 us (26%)
  waiting for transfers between devices  15.3 us (12%)
  starting transfers between devices  14.7 us (12%)
  between operations  14.1 us (11%)
  other arithmetic  2.2 us (2%)
  local copies, waits for them, and re-layouts  1.88 us (1%)
    pallas_call x2, Pallas kernels, flash(): pl.pallas_call(body, out_shape=out, in_specs=[pl.BlockSpec(memory_space=p...  27.7 us
    all_gather x1, blocking collectives, shards(): lax.all_gather(early, 'sp', axis=0, tiled=True, axis_index_groups=column)  27.3 us
    all_to_all x1, blocking collectives, shards(): lax.all_to_all(partial.reshape(ways, rows // ways, -1), 'tp', split_axis=...  18.3 us
    ppermute x1, waiting for transfers between devices, conv_branch(): lax.ppermute(gated_in[-2:], 'sp', [(s, s + 1) for s in range(count - 1)])  13.5 us
    all_to_all x1, starting transfers between devices, shards(): lax.all_to_all(partial_heads, 'sp', split_axis=0, concat_axis=0, tiled=Tr...  6.89 us
    all_to_all x1, starting transfers between devices, shards(): lax.all_to_all(copies, 'sp', split_axis=0, concat_axis=0, tiled=True, axi...  5.77 us
    pallas_call x1, Pallas kernels, merge(): pl.pallas_call(merge_kernel, out_shape=jax.ShapeDtypeStruct((conv_out.sha...  3.66 us
  transfers between devices with their start and end apart: 4, of which 2 were waited for; matrix products, arithmetic and copies ran while one was open for 1% of the time, Pallas kernels for 10%

profile of v2, /device:TPU:480, one launch (start us, length us, event | category | flops | bytes accessed | tf_op | source)
XLA Modules:
  0.0 126.8 jit_solution(1086978931532730819)
XLA Ops:
  6.5 1.8 %pack.1 = (bf16[112,256]{1,0:T(8,128)(2,1)}, bf16[144,256]{1,0:T(8,128)(2,1)}, bf16[8,256,128]{2,1,0:T(8,128)(2,1)}) custom-call(bf16[256,128]{1,0:T(8,128)(2,1)} %q_ref.1, bf16[256,128]{1,0:T(8,128)(2,1)} %k_ref.1, bf16[256,128]{1,0:T(8,128)(2,1)} %v_ref.1), custom_call_target="tpu_custom_call" | custom-call | tf_op jit(solution)/shard_map/pack/pallas_call | solution.py:38
  8.3 0.0 all-gather.2.cloned.1.call-update
  8.3 5.8 %all-to-all-start = ((bf16[8,256,128]{2,1,0:T(8,128)(2,1)}), bf16[8,256,128]{2,1,0:T(8,128)(2,1)S(1)}, u32[]{:S(2)}, u32[]{:S(2)}) async-start(bf16[8,256,128]{2,1,0:T(8,128)(2,1)} %get-tuple-element.10), calls=%async_computation | async-start | bytes 1048576 | tf_op jit(solution)/shard_map/all_to_all | solution.py:299
  14.1 0.6 pad_add_fusion.refs_0_
  14.7 0.0 copy-done.5
  14.7 27.3 %all_gather.7.refs_2_ = bf16[1792,256]{1,0:T(8,128)(2,1)} all-gather(bf16[112,256]{1,0:T(8,128)(2,1)S(1)} %copy-done.5), channel_id=1, replica_groups={{0,4,64,68,128,132,192,196,256,260,320,324,384,388,448,452},{8,12,72,76..., dimensions={0}, use_global_device_ids=true | all-gather | bytes 974848 | tf_op jit(solution)/shard_map/all_gather | solution.py:302
  42.0 0.0 all-to-all-done
  42.0 0.8 copy-done.1
  42.8 12.4 %flash_first.1 = (f32[2,8,2048]{2,1,0:T(8,128)}, f32[2,144,2048]{2,1,0:T(8,128)}) custom-call(s32[4]{0:T(128)} %pad_add_fusion.refs_0_, bf16[2048,128]{1,0:T(8,128)(2,1)} %bitcast.13, bf16[1792,256]{1,0:T(8,128)(2,1)} %all_gather.7.refs_2_), custom_call_target="tpu_custom_call" | custom-call | tf_op jit(solution)/shard_map/flash_first/pallas_call | solution.py:202
  55.2 1.7 %all-gather.2.cloned.1.call-done.refs_2_ = bf16[2304,256]{1,0:T(8,128)(2,1)} async-done(((bf16[144,256]{1,0:T(8,128)(2,1)}), bf16[2304,256]{1,0:T(8,128)(2,1)}) %all-gather.2.cloned.1.call-update) | async-done | bytes 1179664 | tf_op jit(solution)/shard_map/all_gather | solution.py:298
  56.9 15.3 %flash_last.1 = bf16[8,288,256]{2,1,0:T(8,128)(2,1)} custom-call(s32[4]{0:T(128)} %pad_add_fusion.refs_0_, bf16[2048,128]{1,0:T(8,128)(2,1)} %bitcast.14, bf16[2304,256]{1,0:T(8,128)(2,1)} %all-gather.2.cloned.1.call-done.refs_2_, f32[2,8,2048]{2,1,0:T(8,128)} %get-tuple-element.13.refs_3_, f32[2,144,2048]{2,1,0:T(8,128)} %get-tuple-element.14.refs_4_), custom_call_target="tpu_custom_call" | custom-call | tf_op jit(solution)/shard_map/flash_last/pallas_call | solution.py:202
  72.2 0.0 copy-start.2
  72.2 0.0 copy-start.3
  72.2 0.0 copy-start.6
  72.2 0.0 copy-start.4
  72.2 6.9 %all-to-all-start.1 = ((bf16[8,288,256]{2,1,0:T(8,128)(2,1)}), bf16[8,288,256]{2,1,0:T(8,128)(2,1)S(1)}, u32[]{:S(2)}, u32[]{:S(2)}) async-start(bf16[8,288,256]{2,1,0:T(8,128)(2,1)} %flash_last.1), calls=%async_computation.1 | async-start | bytes 2359296 | tf_op jit(solution)/shard_map/all_to_all | solution.py:306
  79.2 2.0 %collective-permute-start = (bf16[2,128]{1,0:T(2,128)(2,1)S(1)}, bf16[2,128]{1,0:T(2,128)(2,1)S(1)}, u32[]{:S(2)}, u32[]{:S(2)}) collective-permute-start(bf16[2,128]{1,0:T(2,128)(2,1)S(1)} %slice.28), channel_id=1, source_target_pairs={{0,4},{4,8},{8,12},{12,16},{16,20},{20,24},{24,28},{28,32},{32,36}... | collective-permute-start | bytes 1544 | tf_op jit(solution)/shard_map/ppermute | solution.py:256
  81.9 13.5 %collective-permute-done = bf16[2,128]{1,0:T(2,128)(2,1)S(1)} collective-permute-done((bf16[2,128]{1,0:T(2,128)(2,1)S(1)}, bf16[2,128]{1,0:T(2,128)(2,1)S(1)}, u32[]{:S(2)}, u32[]{:S(2)}) %collective-permute-start) | collective-permute-done | bytes 544 | tf_op jit(solution)/shard_map/ppermute | solution.py:256
  95.4 0.7 fusion.2.conv
  96.1 0.0 all-to-all-done.1.parts
  96.1 1.0 copy-done
  97.1 3.7 %merge.1 = bf16[256,2048]{1,0:T(8,128)(2,1)} custom-call(f32[1]{0:T(128)S(6)} %copy.12.lam, bf16[8,288,256]{2,1,0:T(8,128)(2,1)} %copy-done, f32[1,128]{1,0:T(1,128)} %bitcast.16, bf16[256,128]{1,0:T(8,128)(2,1)} %fusion.2.conv, bf16[128,2048]{1,0:T(8,128)(2,1)} %w_conv.1, bf16[128,2048]{1,0:T(8,128)(2,1)} %w_heads.1), custom_call_target="tpu_custom_call" | custom-call | tf_op jit(solution)/shard_map/merge/pallas_call | solution.py:244
  100.8 18.3 %all_to_all.15 = bf16[4,64,2048]{2,1,0:T(8,128)(2,1)S(1)} all-to-all(bf16[4,64,2048]{2,1,0:T(8,128)(2,1)} %bitcast.15), channel_id=1, replica_groups=mesh['sp'=128,'tp'=4] {'tp'}, dimensions={0} | all-to-all | bytes 2097152 | tf_op jit(solution)/shard_map/all_to_all | solution.py:311
  119.0 0.9 reduce_sum.12
  (13 shorter events, 0.1 us)
Async XLA Ops:
  6.5 50.4 %all-gather.2.cloned.1.call-start = ((), (), s32[]{:S(2)}) async-start(), calls=%async_computation.3 | async-start | bytes 1253376 | tf_op jit(solution)/shard_map/all_gather | solution.py:298
  8.3 6.4 %copy-start.5 = (bf16[112,256]{1,0:T(8,128)(2,1)S(1)}, bf16[112,256]{1,0:T(8,128)(2,1)}, u32[]{:S(2)}) copy-start(bf16[112,256]{1,0:T(8,128)(2,1)} %get-tuple-element.12) | copy-start | bytes 172036
  8.3 33.6 %all-to-all-start = ((bf16[8,256,128]{2,1,0:T(8,128)(2,1)}), bf16[8,256,128]{2,1,0:T(8,128)(2,1)S(1)}, u32[]{:S(2)}, u32[]{:S(2)}) async-start(bf16[8,256,128]{2,1,0:T(8,128)(2,1)} %get-tuple-element.10), calls=%async_computation | async-start | bytes 1048576 | tf_op jit(solution)/shard_map/all_to_all | solution.py:299
  42.0 0.8 copy-start.1
  72.2 6.9 %copy-start.2 = (bf16[256,128]{1,0:T(8,128)(2,1)S(1)}, bf16[256,128]{1,0:T(8,128)(2,1)}, u32[]{:S(2)}) copy-start(bf16[256,128]{1,0:T(8,128)(2,1)} %param.13) | copy-start | bytes 196612
  72.2 6.9 %copy-start.3 = (bf16[256,128]{1,0:T(8,128)(2,1)S(1)}, bf16[256,128]{1,0:T(8,128)(2,1)}, u32[]{:S(2)}) copy-start(bf16[256,128]{1,0:T(8,128)(2,1)} %param.12) | copy-start | bytes 196612
  72.2 9.0 %copy-start.6 = (bf16[3,128]{1,0:T(4,128)(2,1)S(1)}, bf16[3,128]{1,0:T(4,128)(2,1)}, u32[]{:S(2)}) copy-start(bf16[3,128]{1,0:T(4,128)(2,1)} %param.14) | copy-start | bytes 2308
  72.2 23.2 %copy-start.4 = (bf16[256,128]{1,0:T(8,128)(2,1)S(1)}, bf16[256,128]{1,0:T(8,128)(2,1)}, u32[]{:S(2)}) copy-start(bf16[256,128]{1,0:T(8,128)(2,1)} %param.11) | copy-start | bytes 196612
  72.2 23.8 %all-to-all-start.1 = ((bf16[8,288,256]{2,1,0:T(8,128)(2,1)}), bf16[8,288,256]{2,1,0:T(8,128)(2,1)S(1)}, u32[]{:S(2)}, u32[]{:S(2)}) async-start(bf16[8,288,256]{2,1,0:T(8,128)(2,1)} %flash_last.1), calls=%async_computation.1 | async-start | bytes 2359296 | tf_op jit(solution)/shard_map/all_to_all | solution.py:306
  79.2 16.2 %collective-permute-start = (bf16[2,128]{1,0:T(2,128)(2,1)S(1)}, bf16[2,128]{1,0:T(2,128)(2,1)S(1)}, u32[]{:S(2)}, u32[]{:S(2)}) collective-permute-start(bf16[2,128]{1,0:T(2,128)(2,1)S(1)} %slice.28), channel_id=1, source_target_pairs={{0,4},{4,8},{8,12},{12,16},{16,20},{20,24},{24,28},{28,32},{32,36}... | collective-permute-start | bytes 1544 | tf_op jit(solution)/shard_map/ppermute | solution.py:256
  96.1 1.0 copy-start
Sparse Core Ops, SparseCore 0:
  9.5 47.4 all-gather.1
